TPU v7x, 32 devices: a whole 2x2x4 slice. The times are simulated.
32 devices in a mesh: ep: 8 (over z, x), tp: 4 (over y, core).
Axes of the slice: x: 2, y: 2, z: 4, core: 2. Of those that a mesh axis runs over, the one named last changes fastest.
Arguments:
- tokens: bfloat16 [384, 1024], P('ep'), may hold values from -6 to 6
- head_state: float32 [384, 8, 64, 64], P('ep', 'tp'), may hold values from -6 to 6
- recept_weight: bfloat16 [1024, 512], P(None, 'tp'), may hold values from -0.1875 to 0.1875
- key_weight: bfloat16 [1024, 512], P(None, 'tp'), may hold values from -0.1875 to 0.1875
- value_weight: bfloat16 [1024, 512], P(None, 'tp'), may hold values from -0.1875 to 0.1875
- decay_down_factor: bfloat16 [1024, 64], replicated, may hold values from -0.1875 to 0.1875
- decay_up_factor: bfloat16 [64, 512], P(None, 'tp'), may hold values from -0.75 to 0.75
- decay_base: float32 [512], P('tp'), may hold values from -5 to 3
- rate_down_factor: bfloat16 [1024, 64], replicated, may hold values from -0.1875 to 0.1875
- rate_up_factor: bfloat16 [64, 512], P(None, 'tp'), may hold values from -0.75 to 0.75
- rate_base: float32 [512], P('tp'), may hold values from -3 to 3
- head_gain: float32 [512], P('tp'), may hold values from 0.1 to 1.9
- out_weight: bfloat16 [512, 1024], P('tp'), may hold values from -0.25 to 0.25
- route_experts: int32 [384, 4], P('ep'), may hold values from 0 to 7, all different within a row; in each aligned block of 48 rows (0 to 47, 48 to 95, ...) at most 48 rows name the same one
- route_weights: float32 [384, 4], P('ep'), may hold values from 0.03 to 0.2
- expert_gate: bfloat16 [8, 1024, 1024], P('ep', None, 'tp'), may hold values from -1 to 1
- expert_up: bfloat16 [8, 1024, 1024], P('ep', None, 'tp'), may hold values from -1 to 1
- expert_down: bfloat16 [8, 1024, 1024], P('ep', 'tp'), may hold values from -0.1875 to 0.1875
Outputs:
- layer_out: bfloat16 [384, 1024], P('ep', 'tp')
- new_state: float32 [384, 8, 64, 64], P('ep', 'tp')
Inputs may be any that keep to these rules, and one draw needn't show every extreme that they name: `route_experts`: each row names 4 different experts. In each aligned block of 48 rows no expert is named by more than 48 rows, a bound that some block reaches.
All inputs are finite; a program needn't handle non-finite values.
Results may differ from a plain program's by a relative error of at most 0.02.
Values may be sent and summed in bfloat16 or wider, within the bound.
No kernel may reach another device: no remote copies, remote signals or barrier semaphores. Data moves between devices by JAX's collectives and lax.ppermute only.
A program may use at most 128 MiB of HBM per device.

v0:
```python
import jax
import jax.numpy as jnp
from jax import lax
from jax.sharding import PartitionSpec as P

NORM_EPS = 1e-05
GROUP_EPS = 0.00064
UNIT_EPS = 1e-06
CLAMP_LIMIT = 7.0
GLU_ALPHA = 1.702


def row_norm(values):
    return values * lax.rsqrt(jnp.mean(values * values, axis=-1, keepdims=True) + NORM_EPS)


def clamped_unit(gate_pre, up_pre):
    gated = jnp.minimum(gate_pre, CLAMP_LIMIT)
    linear = jnp.clip(up_pre, -CLAMP_LIMIT, CLAMP_LIMIT)
    return gated * jax.nn.sigmoid(GLU_ALPHA * gated) * (linear + 1.0)


def update_heads(head_state, recept, keys, values, decay_rate, rate_gate, head_gain):
    seq_count, head_count, head_size = head_state.shape[:3]

    def by_heads(operand):
        return operand.astype(jnp.float32).reshape(seq_count, head_count, head_size)

    recept_heads = by_heads(recept)
    key_heads = by_heads(keys)
    value_heads = by_heads(values)
    decay_heads = by_heads(decay_rate)
    rate_heads = by_heads(rate_gate)
    unit_key = key_heads * lax.rsqrt(
        jnp.sum(key_heads * key_heads, axis=-1, keepdims=True) + UNIT_EPS
    )
    highest = lax.Precision.HIGHEST
    state_unit = jnp.einsum("shvk,shk->shv", head_state, unit_key, precision=highest)
    new_state = (
        head_state * decay_heads[:, :, None, :]
        - state_unit[..., None] * (unit_key * rate_heads)[:, :, None, :]
        + value_heads[..., None] * (key_heads * rate_heads)[:, :, None, :]
    )
    head_out = jnp.einsum("shvk,shk->shv", new_state, recept_heads, precision=highest)
    centre = jnp.mean(head_out, axis=-1, keepdims=True)
    spread = jnp.mean(jnp.square(head_out - centre), axis=-1, keepdims=True)
    normed_heads = (head_out - centre) * lax.rsqrt(spread + GROUP_EPS)
    mixed = (normed_heads.reshape(seq_count, -1) * head_gain).astype(jnp.bfloat16)
    return (new_state, mixed)


def local(
    tokens,
    head_state,
    recept_weight,
    key_weight,
    value_weight,
    decay_down_factor,
    decay_up_factor,
    decay_base,
    rate_down_factor,
    rate_up_factor,
    rate_base,
    head_gain,
    out_weight,
    route_experts,
    route_weights,
    expert_gate,
    expert_up,
    expert_down,
):
    tokens_float = tokens.astype(jnp.float32)
    normed = row_norm(tokens_float).astype(jnp.bfloat16)
    recept = jnp.dot(normed, recept_weight, preferred_element_type=jnp.float32).astype(jnp.bfloat16)
    keys = jnp.dot(normed, key_weight, preferred_element_type=jnp.float32).astype(jnp.bfloat16)
    values = jnp.dot(normed, value_weight, preferred_element_type=jnp.float32).astype(jnp.bfloat16)
    decay_low = jnp.tanh(
        jnp.dot(normed, decay_down_factor, preferred_element_type=jnp.float32)
    ).astype(jnp.bfloat16)
    rate_low = jnp.dot(normed, rate_down_factor, preferred_element_type=jnp.float32).astype(
        jnp.bfloat16
    )
    decay_pre = decay_base + jnp.dot(decay_low, decay_up_factor, preferred_element_type=jnp.float32)
    decay_rate = jnp.exp(-jnp.exp(-jax.nn.softplus(-decay_pre) - 0.5))
    rate_gate = jax.nn.sigmoid(
        rate_base + jnp.dot(rate_low, rate_up_factor, preferred_element_type=jnp.float32)
    )
    new_state, mixed = update_heads(
        head_state, recept, keys, values, decay_rate, rate_gate, head_gain
    )
    partial_value = jnp.dot(mixed, out_weight, preferred_element_type=jnp.float32).astype(
        jnp.bfloat16
    )
    partial_value = lax.optimization_barrier(partial_value).astype(jnp.float32)
    summed = lax.psum(partial_value.astype(jnp.bfloat16), "tp").astype(jnp.float32)
    residual = (tokens_float + summed).astype(jnp.bfloat16)
    expert_input = row_norm(residual.astype(jnp.float32)).astype(jnp.bfloat16)
    seq_count, top_count = route_experts.shape
    expert_count = lax.axis_size("ep")
    capacity = max(2, (2 * seq_count * top_count + expert_count - 1) // expert_count)
    column_count = expert_input.shape[1] // lax.axis_size("tp")
    column_start = lax.axis_index("tp") * column_count
    flat_routes = route_experts.reshape(-1)
    onehot = (flat_routes[:, None] == jnp.arange(expert_count, dtype=jnp.int32)[None, :]).astype(
        jnp.int32
    )
    earlier = jnp.cumsum(onehot, axis=0) - onehot
    target = flat_routes * capacity + jnp.sum(earlier * onehot, axis=1)
    slot_ids = jnp.arange(expert_count * capacity, dtype=jnp.int32)
    dispatch_map = jnp.any(
        slot_ids[:, None, None] == target.reshape(seq_count, top_count)[None], axis=-1
    )
    dispatch_map = dispatch_map.astype(jnp.bfloat16)
    outgoing = lax.dynamic_slice_in_dim(expert_input, column_start, column_count, 1)
    buffer = jnp.dot(dispatch_map, outgoing, preferred_element_type=jnp.float32).astype(
        jnp.bfloat16
    )
    buffer = buffer.reshape(expert_count, capacity, outgoing.shape[1])
    slot_rows = lax.all_gather(
        lax.all_to_all(buffer, "ep", split_axis=0, concat_axis=0, tiled=True),
        "tp",
        axis=2,
        tiled=True,
    )
    source_count, slot_count, model_width = slot_rows.shape
    flat_rows = slot_rows.reshape(-1, model_width)
    gate_pre = jnp.dot(flat_rows, expert_gate[0], preferred_element_type=jnp.float32)
    up_pre = jnp.dot(flat_rows, expert_up[0], preferred_element_type=jnp.float32)
    activated = clamped_unit(gate_pre, up_pre).astype(jnp.bfloat16)
    part_out = jnp.dot(activated, expert_down[0], preferred_element_type=jnp.float32).astype(
        jnp.bfloat16
    )
    part_out = lax.optimization_barrier(part_out).astype(jnp.float32)
    part_out = part_out.reshape(source_count, slot_count, model_width)
    shares = lax.psum_scatter(part_out.astype(jnp.bfloat16), "tp", scatter_dimension=2, tiled=True)
    returned = lax.all_to_all(shares, "ep", split_axis=0, concat_axis=0, tiled=True)
    picked = returned.reshape(expert_count * capacity, column_count)[target]
    picked = picked.reshape(seq_count, top_count, column_count).astype(jnp.float32)
    mixture = jnp.sum(route_weights[:, :, None] * picked, axis=1)
    own_residual = lax.dynamic_slice_in_dim(residual, column_start, column_count, 1).astype(
        jnp.float32
    )
    layer_out = (own_residual + mixture).astype(jnp.bfloat16)
    return (layer_out, new_state)


def solution(mesh):
    in_specs = (
        P("ep", None),
        P("ep", "tp", None, None),
        P(None, "tp"),
        P(None, "tp"),
        P(None, "tp"),
        P(),
        P(None, "tp"),
        P("tp"),
        P(),
        P(None, "tp"),
        P("tp"),
        P("tp"),
        P("tp", None),
        P("ep", None),
        P("ep", None),
        P("ep", None, "tp"),
        P("ep", None, "tp"),
        P("ep", "tp", None),
    )
    out_specs = (P("ep", "tp"), P("ep", "tp", None, None))
    return jax.shard_map(local, mesh=mesh, in_specs=in_specs, out_specs=out_specs, check_vma=False)
```

profile of v0, /device:TPU:0, one launch (start us, length us, event | category | flops | bytes accessed | tf_op | source)
XLA Modules:
  0.0 132.7 jit_solution(9616172341950078391)
XLA Ops:
  7.2 0.0 all-reduce.3.cloned.1.call-start
  7.2 1.1 fusion.22
  8.3 1.2 fusion.10
  9.5 0.1 reshape.151
  9.6 0.1 multiply_reduce_fusion.3
  9.8 1.3 %fusion.6 = f32[48,128]{1,0:T(8,128)S(1)} fusion(bf16[64,128]{1,0:T(8,128)(2,1)} %param.27, bf16[1024,64]{0,1:T(8,128)(2,1)} %param.26, f32[128]{0:T(128)} %param.28, bf16[48,1024]{1,0:T(8,128)(2,1)} %param.18, f32[48]{0:T(128)S(1)} %add_rsqrt_fusion.3), kind=kOutput, calls=%fused_computation.14 | convolution fusion | flops 7252992 | bytes 271040 | tf_op jit(solution)/shard_map/dot_general | solution.py:86
  11.1 0.1 reshape.142
  11.2 1.4 %fusion.35 = f32[48,128]{1,0:T(8,128)S(1)} fusion(bf16[64,128]{1,0:T(8,128)(2,1)} %param.24, bf16[1024,64]{0,1:T(8,128)(2,1)} %param.23, f32[128]{0:T(128)} %param.25, bf16[48,1024]{1,0:T(8,128)(2,1)} %param.18, f32[48]{0:T(128)S(1)} %add_rsqrt_fusion.3), kind=kOutput, calls=%fused_computation.59 | convolution fusion | flops 7296000 | bytes 271040 | tf_op jit(solution)/shard_map/dot_general | solution.py:83
  12.6 0.1 mul.155
  12.7 1.2 fusion.9
  13.9 0.1 reshape.152
  14.0 1.2 convolution_convert_fusion.3
  15.2 0.1 reshape.168
  15.3 0.1 fusion.54
  15.5 7.0 %fusion.55 = f32[48,2,1,64]{3,2,1,0:T(1,128)S(1)} fusion(f32[48,2,64,1]{2,3,1,0:T(1,128)S(1)} %bitcast.53, f32[48,2,64,64]{3,2,1,0:T(8,128)} %param.19), kind=kOutput, calls=%fused_computation.87 | convolution fusion | flops 4718592 | bytes 1622016 | tf_op jit(solution)/shard_map/shvk,shk->shv/dot_general | solution.py:38
  22.5 2.1 %multiply_add_fusion = f32[48,2,64,64]{3,2,1,0:T(8,128)S(1)} fusion(f32[48,2,64,64]{3,2,1,0:T(8,128)S(1)} %copy-done.1, f32[48,2,64]{2,1,0:T(2,128)S(1)} %get-tuple-element.6, f32[48,2,64]{2,1,0:T(2,128)S(1)} %reshape.152, f32[48,2,64]{2,1,0:T(2,128)S(1)} %get-tuple-element.4, f32[48,2,64]{2,1,0:T(2,128)S(1)} %bitcast.52, f32[48,2,64]{2,1,0:T(2,128)S(1)} %mul.155), kind=kLoop, calls=%fused_computation.1 | loop fusion | flops 1966080 | bytes 3268608 | tf_op jit(solution)/shard_map/add | solution.py:40
  24.6 1.7 %copy-done.2 = f32[48,2,64,64]{3,2,1,0:T(8,128)} copy-done((f32[48,2,64,64]{3,2,1,0:T(8,128)}, f32[48,2,64,64]{3,2,1,0:T(8,128)S(1)}, u32[]{:S(2)}) %copy-start.2) | copy-done | bytes 1572888
  26.2 2.5 %fusion.56 = f32[48,2,1,64]{3,2,1,0:T(1,128)S(1)} fusion(f32[48,2,64,64]{3,2,1,0:T(8,128)S(1)} %multiply_add_fusion, bf16[48,2,64,1]{2,3,1,0:T(2,128)(2,1)S(1)} %reshape.168), kind=kOutput, calls=%fused_computation.88 | convolution fusion | flops 4718592 | bytes 1609728 | tf_op jit(solution)/shard_map/shvk,shk->shv/dot_general | solution.py:44
  28.8 0.1 reduce_sum.69
  28.9 0.2 multiply_reduce_fusion.2
  29.2 0.2 subtract_multiply_fusion
  29.3 0.1 reshape.144
  29.4 0.8 convolution_convert_fusion.2
  30.2 0.0 all-reduce.3.cloned.1.call-update
  30.3 0.0 reduce-scatter.2.cloned.1.call-start
  30.3 0.1 copy.34
  30.4 0.1 eq.36
  30.6 0.6 reduce-window.6
  31.1 0.2 slice_reduce_fusion
  31.4 0.1 add_bitcast_fusion
  31.5 0.1 reduce_sum.72
  31.6 0.1 copy.36
  31.7 0.1 fusion.21
  31.8 33.0 %all-reduce.3.cloned.1.call-done = bf16[48,1024]{1,0:T(8,128)(2,1)} async-done(((bf16[48,1024]{1,0:T(8,128)(2,1)}), bf16[48,1024]{1,0:T(8,128)(2,1)}) %all-reduce.3.cloned.1.call-update) | async-done | bytes 98320 | tf_op jit(solution)/shard_map/psum | solution.py:95
  64.8 1.0 multiply_reduce_fusion.1
  65.9 0.3 convolution_convert_fusion.1
  66.2 13.1 %all_to_all.10 = bf16[8,48,256]{2,1,0:T(8,128)(2,1)S(1)} all-to-all(bf16[8,48,256]{2,1,0:T(8,128)(2,1)S(1)} %bitcast.48), channel_id=1, replica_groups=mesh['ep'=8,'tp'=4] {'ep'}, dimensions={0} | all-to-all | bytes 393216 | tf_op jit(solution)/shard_map/all_to_all | solution.py:120
  79.3 7.6 %all_gather.3 = bf16[8,48,1024]{2,1,0:T(8,128)(2,1)S(1)} all-gather(bf16[8,48,256]{2,1,0:T(8,128)(2,1)S(1)} %all_to_all.10), channel_id=1, replica_groups=mesh['ep'=8,'tp'=4] {'tp'}, dimensions={2}, use_global_device_ids=true | all-gather | bytes 983040 | tf_op jit(solution)/shard_map/all_gather | solution.py:119
  86.9 0.4 convolution_minimum_fusion
  87.3 1.9 %convolution_convert_fusion = bf16[384,1024]{1,0:T(8,128)(2,1)} fusion(bf16[384,1024]{1,0:T(8,128)(2,1)S(1)} %bitcast.46, bf16[1,256,1024]{2,1,0:T(8,128)(2,1)S(1)} %copy-done, bf16[1,1024,256]{2,1,0:T(8,128)(2,1)S(1)} %copy-done.9, f32[384,256]{1,0:T(8,128)S(1)} %convolution_minimum_fusion), kind=kOutput, calls=%fused_computation.2 | convolution fusion | flops 403931136 | bytes 3014656 | tf_op jit(solution)/shard_map/dot_general | solution.py:130
  89.2 21.5 %reduce-scatter.2.cloned.1.call-done = bf16[8,48,256]{2,1,0:T(8,128)(2,1)} async-done(((bf16[8,48,1024]{2,1,0:T(8,128)(2,1)}), bf16[8,48,256]{2,1,0:T(8,128)(2,1)}) %reduce-scatter.2.cloned.1.call-update) | async-done | bytes 196624 | tf_op jit(solution)/shard_map/reduce_scatter | solution.py:135
  110.6 5.5 %all-to-all-start.1 = ((bf16[8,48,256]{2,1,0:T(8,128)(2,1)}), bf16[8,48,256]{2,1,0:T(8,128)(2,1)S(1)}, u32[]{:S(2)}, u32[]{:S(2)}) async-start(bf16[8,48,256]{2,1,0:T(8,128)(2,1)} %reduce-scatter.2.cloned.1.call-done), calls=%async_computation.2 | async-start | bytes 393216 | tf_op jit(solution)/shard_map/all_to_all | solution.py:136
  116.2 0.1 mul.187
  116.3 0.1 copy.33
  116.4 7.6 %all-to-all-done.1 = bf16[8,48,256]{2,1,0:T(8,128)(2,1)S(1)} async-done(((bf16[8,48,256]{2,1,0:T(8,128)(2,1)}), bf16[8,48,256]{2,1,0:T(8,128)(2,1)S(1)}, u32[]{:S(2)}, u32[]{:S(2)}) %all-to-all-start.1) | async-done | bytes 196640 | tf_op jit(solution)/shard_map/all_to_all | solution.py:136
  123.9 1.0 gather_fusion
  125.0 0.2 multiply_reduce_fusion
  125.2 0.6 add_convert_fusion
  (35 shorter events, 0.3 us)
Async XLA Ops:
  7.2 80.1 %copy-start = (bf16[1,256,1024]{2,1,0:T(8,128)(2,1)S(1)}, bf16[1,256,1024]{2,1,0:T(8,128)(2,1)}, u32[]{:S(2)}) copy-start(bf16[1,256,1024]{2,1,0:T(8,128)(2,1)} %param.35) | copy-start | bytes 1572868
  7.2 57.6 %all-reduce.3.cloned.1.call-start = ((), (), s32[]{:S(2)}) async-start(), calls=%async_computation.3 | async-start | bytes 196608 | tf_op jit(solution)/shard_map/psum | solution.py:95
  15.3 7.2 %copy-start.1 = (f32[48,2,64,64]{3,2,1,0:T(8,128)S(1)}, f32[48,2,64,64]{3,2,1,0:T(8,128)}, u32[]{:S(2)}) copy-start(f32[48,2,64,64]{3,2,1,0:T(8,128)} %param.19) | copy-start | bytes 4718596
  24.6 1.7 %copy-start.2 = (f32[48,2,64,64]{3,2,1,0:T(8,128)}, f32[48,2,64,64]{3,2,1,0:T(8,128)S(1)}, u32[]{:S(2)}) copy-start(f32[48,2,64,64]{3,2,1,0:T(8,128)S(1)} %multiply_add_fusion) | copy-start | bytes 4718596
  26.2 3.2 %copy-start.5 = (bf16[128,1024]{1,0:T(8,128)(2,1)S(1)}, bf16[128,1024]{1,0:T(8,128)(2,1)}, u32[]{:S(2)}) copy-start(bf16[128,1024]{1,0:T(8,128)(2,1)} %param.30) | copy-start | bytes 786436
  26.2 3.2 %copy-start.8 = (f32[128]{0:T(128)S(1)}, f32[128]{0:T(128)}, u32[]{:S(2)}) copy-start(f32[128]{0:T(128)} %param.29) | copy-start | bytes 1540
  26.2 4.1 %copy-start.6 = (s32[48,4]{0,1:T(4,128)S(1)}, s32[48,4]{0,1:T(4,128)}, u32[]{:S(2)}) copy-start(s32[48,4]{0,1:T(4,128)} %param.31) | copy-start | bytes 2308
  26.2 38.6 %copy-start.3 = (bf16[48,1024]{1,0:T(8,128)(2,1)S(1)}, bf16[48,1024]{1,0:T(8,128)(2,1)}, u32[]{:S(2)}) copy-start(bf16[48,1024]{1,0:T(8,128)(2,1)} %param.18) | copy-start | bytes 294916
  26.2 60.6 %copy-start.4 = (bf16[1,1024,256]{2,1,0:T(8,128)(2,1)S(1)}, bf16[1,1024,256]{2,1,0:T(8,128)(2,1)}, u32[]{:S(2)}) copy-start(bf16[1,1024,256]{2,1,0:T(8,128)(2,1)} %param.33) | copy-start | bytes 1572868
  28.8 58.5 %copy-start.9 = (bf16[1,1024,256]{2,1,0:T(8,128)(2,1)S(1)}, bf16[1,1024,256]{2,1,0:T(8,128)(2,1)}, u32[]{:S(2)}) copy-start(bf16[1,1024,256]{2,1,0:T(8,128)(2,1)} %param.34) | copy-start | bytes 1572868
  30.3 80.4 %reduce-scatter.2.cloned.1.call-start = ((), (), s32[]{:S(2)}) async-start(), calls=%async_computation.4 | async-start | bytes 983040 | tf_op jit(solution)/shard_map/reduce_scatter | solution.py:135
  87.3 29.0 %copy-start.7 = (f32[48,4]{0,1:T(4,128)S(1)}, f32[48,4]{0,1:T(4,128)}, u32[]{:S(2)}) copy-start(f32[48,4]{0,1:T(4,128)} %param.32) | copy-start | bytes 2308
  110.6 13.3 %all-to-all-start.1 = ((bf16[8,48,256]{2,1,0:T(8,128)(2,1)}), bf16[8,48,256]{2,1,0:T(8,128)(2,1)S(1)}, u32[]{:S(2)}, u32[]{:S(2)}) async-start(bf16[8,48,256]{2,1,0:T(8,128)(2,1)} %reduce-scatter.2.cloned.1.call-done), calls=%async_computation.2 | async-start | bytes 393216 | tf_op jit(solution)/shard_map/all_to_all | solution.py:136
Sparse Core Ops, SparseCore 0:
  30.4 34.3 all-reduce.2
  89.3 21.2 reduce-scatter.1
where the time goes:
time: 133 us
  waiting for transfers between devices  62 us (47%)
  blocking collectives  20.7 us (16%)
  matrix products  19.3 us (15%)
  between operations  14.4 us (11%)
  other arithmetic  6.64 us (5%)
  starting transfers between devices  5.59 us (4%)
  local copies, waits for them, and re-layouts  4.08 us (3%)
    psum x1, waiting for transfers between devices, local(): lax.psum(partial_value.astype(jnp.bfloat16), 'tp').astype(jnp.float32)  33 us
    reduce_scatter x1, waiting for transfers between devices, local(): lax.psum_scatter(part_out.astype(jnp.bfloat16), 'tp', scatter_dimension=2...  21.5 us
    all_to_all x1, blocking collectives, local(): lax.all_to_all(buffer, 'ep', split_axis=0, concat_axis=0, tiled=True)  13.1 us
    all_gather x1, blocking collectives, local(): lax.all_gather(lax.all_to_all(buffer, 'ep', split_axis=0, concat_axis=0,...  7.58 us
    all_to_all x1, waiting for transfers between devices, local(): lax.all_to_all(shares, 'ep', split_axis=0, concat_axis=0, tiled=True)  7.57 us
    dot_general x1, matrix products, update_heads(): jnp.einsum('shvk,shk->shv', head_state, unit_key, precision=highest)  7.01 us
    all_to_all x1, starting transfers between devices, local(): lax.all_to_all(shares, 'ep', split_axis=0, concat_axis=0, tiled=True)  5.51 us
  transfers between devices with their start and end apart: 3, of which 3 were waited for; matrix products, arithmetic and copies ran while one was open for 1% of the time, Pallas kernels for 0%

commit v1 on v0

--- a/solution.py
+++ b/solution.py
@@ -92,7 +92,9 @@
         jnp.bfloat16
     )
     partial_value = lax.optimization_barrier(partial_value).astype(jnp.float32)
-    summed = lax.psum(partial_value.astype(jnp.bfloat16), "tp").astype(jnp.float32)
+    summed = jnp.sum(lax.all_gather(partial_value.astype(jnp.bfloat16), "tp"), axis=0).astype(
+        jnp.float32
+    )
     residual = (tokens_float + summed).astype(jnp.bfloat16)
     expert_input = row_norm(residual.astype(jnp.float32)).astype(jnp.bfloat16)
     seq_count, top_count = route_experts.shape

time: 133 us -> 108 us (0.81)
  waiting for transfers between devices: 62 us -> 28.9 us
  blocking collectives: 20.7 us -> 30.3 us
    psum x1 -> x0, waiting for transfers between devices: 33 us -> none  [local(): lax.psum(partial_value.astype(jnp.bfloat16), 'tp').astype(jnp.float32)]
    all_gather x0 -> x1, blocking collectives: none -> 7.96 us  [local(): lax.all_gather(partial_value.astype(jnp.bfloat16), 'tp')]
  transfers between devices with their start and end apart: 3 -> 2, of which waited for: 3 -> 2; matrix products, arithmetic and copies ran while one was open for 1% -> 0% of each run, Pallas kernels for 0% -> 0%
where the time goes in v1:
time: 108 us
  blocking collectives  30.3 us (28%)
  waiting for transfers between devices  28.9 us (27%)
  matrix products  18.6 us (17%)
  between operations  14.4 us (13%)
  other arithmetic  5.8 us (5%)
  starting transfers between devices  5.57 us (5%)
  local copies, waits for them, and re-layouts  4.08 us (4%)
    reduce_scatter x1, waiting for transfers between devices, local(): lax.psum_scatter(part_out.astype(jnp.bfloat16), 'tp', scatter_dimension=2...  21.3 us
    all_to_all x1, blocking collectives, local(): lax.all_to_all(buffer, 'ep', split_axis=0, concat_axis=0, tiled=True)  14.1 us
    all_gather x1, blocking collectives, local(): lax.all_gather(lax.all_to_all(buffer, 'ep', split_axis=0, concat_axis=0,...  8.26 us
    all_gather x1, blocking collectives, local(): lax.all_gather(partial_value.astype(jnp.bfloat16), 'tp')  7.96 us
    all_to_all x1, waiting for transfers between devices, local(): lax.all_to_all(shares, 'ep', split_axis=0, concat_axis=0, tiled=True)  7.56 us
    dot_general x1, matrix products, update_heads(): jnp.einsum('shvk,shk->shv', head_state, unit_key, precision=highest)  7.01 us
    all_to_all x1, starting transfers between devices, local(): lax.all_to_all(shares, 'ep', split_axis=0, concat_axis=0, tiled=True)  5.53 us
    dot_general x1, matrix products, update_heads(): jnp.einsum('shvk,shk->shv', new_state, recept_heads, precision=highest)  2.55 us
  transfers between devices with their start and end apart: 2, of which 2 were waited for; matrix products, arithmetic and copies ran while one was open for 0% of the time, Pallas kernels for 0%

profile of v1, /device:TPU:0, one launch (start us, length us, event | category | flops | bytes accessed | tf_op | source)
XLA Modules:
  0.0 107.6 jit_solution(3199308004516936415)
XLA Ops:
  7.2 0.0 reduce-scatter.2.cloned.1.call-start
  7.2 1.1 fusion.22
  8.3 1.2 %fusion.10 = f32[48,128]{1,0:T(8,128)S(1)} fusion(bf16[1024,128]{1,0:T(8,128)(2,1)} %param.21, bf16[48,1024]{1,0:T(8,128)(2,1)} %param.18, f32[48]{0:T(128)S(1)} %add_rsqrt_fusion.3), kind=kOutput, calls=%fused_computation.24 | convolution fusion | flops 12742656 | bytes 385216 | tf_op jit(solution)/shard_map/dot_general | solution.py:75
  9.5 0.1 reshape.151
  9.6 0.1 multiply_reduce_fusion.3
  9.8 1.3 %fusion.6 = f32[48,128]{1,0:T(8,128)S(1)} fusion(bf16[64,128]{1,0:T(8,128)(2,1)} %param.27, bf16[1024,64]{0,1:T(8,128)(2,1)} %param.26, f32[128]{0:T(128)} %param.28, bf16[48,1024]{1,0:T(8,128)(2,1)} %param.18, f32[48]{0:T(128)S(1)} %add_rsqrt_fusion.3), kind=kOutput, calls=%fused_computation.14 | convolution fusion | flops 7252992 | bytes 271040 | tf_op jit(solution)/shard_map/dot_general | solution.py:86
  11.1 0.1 reshape.142
  11.2 1.4 %fusion.35 = f32[48,128]{1,0:T(8,128)S(1)} fusion(bf16[64,128]{1,0:T(8,128)(2,1)} %param.24, bf16[1024,64]{0,1:T(8,128)(2,1)} %param.23, f32[128]{0:T(128)} %param.25, bf16[48,1024]{1,0:T(8,128)(2,1)} %param.18, f32[48]{0:T(128)S(1)} %add_rsqrt_fusion.3), kind=kOutput, calls=%fused_computation.59 | convolution fusion | flops 7296000 | bytes 271040 | tf_op jit(solution)/shard_map/dot_general | solution.py:83
  12.6 0.1 mul.155
  12.7 1.2 %fusion.9 = f32[48,128]{1,0:T(8,128)S(1)} fusion(bf16[1024,128]{1,0:T(8,128)(2,1)} %param.22, bf16[48,1024]{1,0:T(8,128)(2,1)} %param.18, f32[48]{0:T(128)S(1)} %add_rsqrt_fusion.3), kind=kOutput, calls=%fused_computation.21 | convolution fusion | flops 12742656 | bytes 385216 | tf_op jit(solution)/shard_map/dot_general | solution.py:76
  13.9 0.1 reshape.152
  14.0 1.2 %convolution_convert_fusion.3 = bf16[48,128]{1,0:T(8,128)(2,1)S(1)} fusion(bf16[1024,128]{1,0:T(8,128)(2,1)} %param.20, bf16[48,1024]{1,0:T(8,128)(2,1)} %param.18, f32[48]{0:T(128)S(1)} %add_rsqrt_fusion.3), kind=kOutput, calls=%fused_computation.19 | convolution fusion | flops 12736512 | bytes 372928 | tf_op jit(solution)/shard_map/dot_general | solution.py:74
  15.3 0.1 reshape.169
  15.4 0.1 fusion.54
  15.5 7.0 %fusion.55 = f32[48,2,1,64]{3,2,1,0:T(1,128)S(1)} fusion(f32[48,2,64,1]{2,3,1,0:T(1,128)S(1)} %bitcast.55, f32[48,2,64,64]{3,2,1,0:T(8,128)} %param.19), kind=kOutput, calls=%fused_computation.87 | convolution fusion | flops 4718592 | bytes 1622016 | tf_op jit(solution)/shard_map/shvk,shk->shv/dot_general | solution.py:38
  22.5 2.1 %multiply_add_fusion = f32[48,2,64,64]{3,2,1,0:T(8,128)S(1)} fusion(f32[48,2,64,64]{3,2,1,0:T(8,128)S(1)} %copy-done.1, f32[48,2,64]{2,1,0:T(2,128)S(1)} %get-tuple-element.6, f32[48,2,64]{2,1,0:T(2,128)S(1)} %reshape.152, f32[48,2,64]{2,1,0:T(2,128)S(1)} %get-tuple-element.4, f32[48,2,64]{2,1,0:T(2,128)S(1)} %bitcast.54, f32[48,2,64]{2,1,0:T(2,128)S(1)} %mul.155), kind=kLoop, calls=%fused_computation.1 | loop fusion | flops 1966080 | bytes 3268608 | tf_op jit(solution)/shard_map/add | solution.py:40
  24.6 1.7 %copy-done.2 = f32[48,2,64,64]{3,2,1,0:T(8,128)} copy-done((f32[48,2,64,64]{3,2,1,0:T(8,128)}, f32[48,2,64,64]{3,2,1,0:T(8,128)S(1)}, u32[]{:S(2)}) %copy-start.2) | copy-done | bytes 1572888
  26.2 2.5 %fusion.56 = f32[48,2,1,64]{3,2,1,0:T(1,128)S(1)} fusion(f32[48,2,64,64]{3,2,1,0:T(8,128)S(1)} %multiply_add_fusion, bf16[48,2,64,1]{2,3,1,0:T(2,128)(2,1)S(1)} %reshape.169), kind=kOutput, calls=%fused_computation.88 | convolution fusion | flops 4718592 | bytes 1609728 | tf_op jit(solution)/shard_map/shvk,shk->shv/dot_general | solution.py:44
  28.8 0.1 reduce_sum.81
  28.9 0.2 multiply_reduce_fusion.2
  29.2 0.2 subtract_multiply_fusion
  29.3 0.1 reshape.144
  29.4 0.2 convolution_convert_fusion.2
  29.6 8.0 %all-gather = bf16[192,1024]{1,0:T(8,128)(2,1)S(1)} all-gather(bf16[48,1024]{1,0:T(8,128)(2,1)S(1)} %convolution_convert_fusion.2), channel_id=2, replica_groups=mesh['ep'=8,'tp'=4] {'tp'}, dimensions={0}, use_global_device_ids=true | all-gather | bytes 491520 | tf_op jit(solution)/shard_map/all_gather | solution.py:95
  37.6 0.1 reduce_sum.83
  37.7 0.1 multiply_reduce_fusion.1
  37.8 0.1 copy.34
  37.9 0.1 eq.36
  38.1 0.6 reduce-window.6
  38.6 0.2 slice_reduce_fusion
  38.9 0.1 add_bitcast_fusion
  39.0 0.1 reduce_sum.85
  39.1 0.1 copy.36
  39.2 0.1 fusion.21
  39.3 0.3 convolution_convert_fusion.1
  39.6 14.1 %all_to_all.10 = bf16[8,48,256]{2,1,0:T(8,128)(2,1)S(1)} all-to-all(bf16[8,48,256]{2,1,0:T(8,128)(2,1)S(1)} %bitcast.50), channel_id=1, replica_groups=mesh['ep'=8,'tp'=4] {'ep'}, dimensions={0} | all-to-all | bytes 393216 | tf_op jit(solution)/shard_map/all_to_all | solution.py:122
  53.7 8.3 %all_gather.11 = bf16[8,48,1024]{2,1,0:T(8,128)(2,1)S(1)} all-gather(bf16[8,48,256]{2,1,0:T(8,128)(2,1)S(1)} %all_to_all.10), channel_id=1, replica_groups=mesh['ep'=8,'tp'=4] {'tp'}, dimensions={2}, use_global_device_ids=true | all-gather | bytes 983040 | tf_op jit(solution)/shard_map/all_gather | solution.py:121
  62.0 0.4 convolution_minimum_fusion
  62.4 1.9 %convolution_convert_fusion = bf16[384,1024]{1,0:T(8,128)(2,1)} fusion(bf16[384,1024]{1,0:T(8,128)(2,1)S(1)} %bitcast.47, bf16[1,256,1024]{2,1,0:T(8,128)(2,1)S(1)} %copy-done, bf16[1,1024,256]{2,1,0:T(8,128)(2,1)S(1)} %copy-done.9, f32[384,256]{1,0:T(8,128)S(1)} %convolution_minimum_fusion), kind=kOutput, calls=%fused_computation.2 | convolution fusion | flops 403931136 | bytes 3014656 | tf_op jit(solution)/shard_map/dot_general | solution.py:132
  64.2 0.0 reduce-scatter.2.cloned.1.call-update
  64.3 21.3 %reduce-scatter.2.cloned.1.call-done = bf16[8,48,256]{2,1,0:T(8,128)(2,1)} async-done(((bf16[8,48,1024]{2,1,0:T(8,128)(2,1)}), bf16[8,48,256]{2,1,0:T(8,128)(2,1)}) %reduce-scatter.2.cloned.1.call-update) | async-done | bytes 196624 | tf_op jit(solution)/shard_map/reduce_scatter | solution.py:137
  85.6 5.5 %all-to-all-start.1 = ((bf16[8,48,256]{2,1,0:T(8,128)(2,1)}), bf16[8,48,256]{2,1,0:T(8,128)(2,1)S(1)}, u32[]{:S(2)}, u32[]{:S(2)}) async-start(bf16[8,48,256]{2,1,0:T(8,128)(2,1)} %reduce-scatter.2.cloned.1.call-done), calls=%async_computation.2 | async-start | bytes 393216 | tf_op jit(solution)/shard_map/all_to_all | solution.py:138
  91.1 0.1 mul.187
  91.2 0.1 copy.33
  91.3 7.6 %all-to-all-done.1 = bf16[8,48,256]{2,1,0:T(8,128)(2,1)S(1)} async-done(((bf16[8,48,256]{2,1,0:T(8,128)(2,1)}), bf16[8,48,256]{2,1,0:T(8,128)(2,1)S(1)}, u32[]{:S(2)}, u32[]{:S(2)}) %all-to-all-start.1) | async-done | bytes 196640 | tf_op jit(solution)/shard_map/all_to_all | solution.py:138
  98.9 1.0 gather_fusion
  99.9 0.2 multiply_reduce_fusion
  100.1 0.6 add_convert_fusion
  (34 shorter events, 0.3 us)
Async XLA Ops:
  7.2 55.2 %copy-start = (bf16[1,256,1024]{2,1,0:T(8,128)(2,1)S(1)}, bf16[1,256,1024]{2,1,0:T(8,128)(2,1)}, u32[]{:S(2)}) copy-start(bf16[1,256,1024]{2,1,0:T(8,128)(2,1)} %param.35) | copy-start | bytes 1572868
  7.2 78.4 %reduce-scatter.2.cloned.1.call-start = ((), (), s32[]{:S(2)}) async-start(), calls=%async_computation.3 | async-start | bytes 983040 | tf_op jit(solution)/shard_map/reduce_scatter | solution.py:137
  15.3 7.1 %copy-start.1 = (f32[48,2,64,64]{3,2,1,0:T(8,128)S(1)}, f32[48,2,64,64]{3,2,1,0:T(8,128)}, u32[]{:S(2)}) copy-start(f32[48,2,64,64]{3,2,1,0:T(8,128)} %param.19) | copy-start | bytes 4718596
  24.6 1.7 %copy-start.2 = (f32[48,2,64,64]{3,2,1,0:T(8,128)}, f32[48,2,64,64]{3,2,1,0:T(8,128)S(1)}, u32[]{:S(2)}) copy-start(f32[48,2,64,64]{3,2,1,0:T(8,128)S(1)} %multiply_add_fusion) | copy-start | bytes 4718596
  26.2 3.2 %copy-start.5 = (bf16[128,1024]{1,0:T(8,128)(2,1)S(1)}, bf16[128,1024]{1,0:T(8,128)(2,1)}, u32[]{:S(2)}) copy-start(bf16[128,1024]{1,0:T(8,128)(2,1)} %param.30) | copy-start | bytes 786436
  26.2 3.2 %copy-start.8 = (f32[128]{0:T(128)S(1)}, f32[128]{0:T(128)}, u32[]{:S(2)}) copy-start(f32[128]{0:T(128)} %param.29) | copy-start | bytes 1540
  26.2 11.4 %copy-start.3 = (bf16[48,1024]{1,0:T(8,128)(2,1)S(1)}, bf16[48,1024]{1,0:T(8,128)(2,1)}, u32[]{:S(2)}) copy-start(bf16[48,1024]{1,0:T(8,128)(2,1)} %param.18) | copy-start | bytes 294916
  26.2 11.6 %copy-start.6 = (s32[48,4]{0,1:T(4,128)S(1)}, s32[48,4]{0,1:T(4,128)}, u32[]{:S(2)}) copy-start(s32[48,4]{0,1:T(4,128)} %param.31) | copy-start | bytes 2308
  26.2 35.7 %copy-start.4 = (bf16[1,1024,256]{2,1,0:T(8,128)(2,1)S(1)}, bf16[1,1024,256]{2,1,0:T(8,128)(2,1)}, u32[]{:S(2)}) copy-start(bf16[1,1024,256]{2,1,0:T(8,128)(2,1)} %param.33) | copy-start | bytes 1572868
  28.8 33.6 %copy-start.9 = (bf16[1,1024,256]{2,1,0:T(8,128)(2,1)S(1)}, bf16[1,1024,256]{2,1,0:T(8,128)(2,1)}, u32[]{:S(2)}) copy-start(bf16[1,1024,256]{2,1,0:T(8,128)(2,1)} %param.34) | copy-start | bytes 1572868
  62.4 28.8 %copy-start.7 = (f32[48,4]{0,1:T(4,128)S(1)}, f32[48,4]{0,1:T(4,128)}, u32[]{:S(2)}) copy-start(f32[48,4]{0,1:T(4,128)} %param.32) | copy-start | bytes 2308
  85.6 13.3 %all-to-all-start.1 = ((bf16[8,48,256]{2,1,0:T(8,128)(2,1)}), bf16[8,48,256]{2,1,0:T(8,128)(2,1)S(1)}, u32[]{:S(2)}, u32[]{:S(2)}) async-start(bf16[8,48,256]{2,1,0:T(8,128)(2,1)} %reduce-scatter.2.cloned.1.call-done), calls=%async_computation.2 | async-start | bytes 393216 | tf_op jit(solution)/shard_map/all_to_all | solution.py:138
Sparse Core Ops, SparseCore 0:
  64.4 21.1 reduce-scatter.1
